TPU v7x, 32 devices: a whole 2x2x4 slice. The times are simulated.
32 devices in a mesh: sp: 8 (over z, x), tp: 4 (over y, core).
Axes of the slice: x: 2, y: 2, z: 4, core: 2. Of those that a mesh axis runs over, the one named last changes fastest.
Arguments:
- tokens: bfloat16 [4096, 2048], P('sp', 'tp'), may hold values from -6 to 6
- norm_gain: float32 [2048], replicated, may hold values from 0.1 to 1.9
- w_query: bfloat16 [2048, 1024], P('sp', 'tp'), may hold values from -1 to 1
- w_key: bfloat16 [2048, 256], P('sp', 'tp'), may hold values from -16 to 16
- w_value: bfloat16 [2048, 256], P('sp', 'tp'), may hold values from -1 to 1
- w_post_gate: bfloat16 [2048, 1024], P('sp', 'tp'), may hold values from -0.125 to 0.125
- w_pre_gate: bfloat16 [2048, 1024], P('sp', 'tp'), may hold values from -0.125 to 0.125
- w_conv_in: bfloat16 [2048, 1024], P('sp', 'tp'), may hold values from -0.125 to 0.125
- conv_taps: float32 [3, 1024], P(None, 'tp'), may hold values from -3 to 3
- sink_logit: float32 [16], P('tp'), may hold values from 2 to 6
- w_out_attn: bfloat16 [1024, 2048], P('tp', 'sp'), may hold values from -0.1875 to 0.1875
- w_out_conv: bfloat16 [1024, 2048], P('tp', 'sp'), may hold values from -0.1875 to 0.1875
Outputs:
- mixed: bfloat16 [4096, 2048], P(('sp', 'tp'))
- log_weight_sum: float32 [16, 4096], P('tp', 'sp')
All inputs are finite; a program needn't handle non-finite values.
Results may differ from a plain program's by a relative error of at most 0.012.
The roundings to bfloat16 on the way count: a program that leaves them out, or rounds other values in their place, can miss the bound.
Values may be sent and summed in bfloat16 or wider, within the bound.
A program may use at most 64 MiB of HBM per device.

v0:
```python
import jax
import jax.numpy as jnp
from jax import lax
from jax.sharding import PartitionSpec as P

HEAD_DIM = 64
WINDOW = 128
GRID_W = 64


rope_base = 10000.0
norm_eps = 1e-06


def padded(block, sides, width):
    for axis, dim in sides:
        count = lax.axis_size(axis)
        forward = [(i, i + 1) for i in range(count - 1)]
        backward = [(target, source) for source, target in forward]
        low = lax.ppermute(
            lax.slice_in_dim(block, block.shape[dim] - width, None, axis=dim), axis, forward
        )
        high = lax.ppermute(lax.slice_in_dim(block, 0, width, axis=dim), axis, backward)
        block = jnp.concatenate([low, block, high], axis=dim)
    return block


def rotate_pair(values, angles):
    first_half, second_half = jnp.split(values, 2, axis=-1)
    cosine = jnp.cos(angles)[:, None, :]
    sine_part = jnp.sin(angles)[:, None, :]
    return jnp.concatenate(
        [
            first_half * cosine - second_half * sine_part,
            first_half * sine_part + second_half * cosine,
        ],
        axis=-1,
    )


def axial_rotate(values, positions):
    half_dim = values.shape[-1] // 2
    inv_freq = rope_base ** (-jnp.arange(0, half_dim, 2).astype(jnp.float32) / half_dim)
    row_angle = (positions // GRID_W).astype(jnp.float32)[:, None] * inv_freq
    col_angle = (positions % GRID_W).astype(jnp.float32)[:, None] * inv_freq
    row_part, col_part = jnp.split(values, 2, axis=-1)
    return jnp.concatenate(
        [rotate_pair(row_part, row_angle), rotate_pair(col_part, col_angle)], axis=-1
    )


def block_windows(source, rows_local, blocks):
    pieces = [
        source[step * WINDOW : step * WINDOW + rows_local].reshape(
            (blocks, WINDOW) + source.shape[1:]
        )
        for step in range(3)
    ]
    return jnp.concatenate(pieces, axis=1)


def on_device(
    tokens,
    norm_gain,
    w_query,
    w_key,
    w_value,
    w_post_gate,
    w_pre_gate,
    w_conv_in,
    conv_taps,
    sink_logit,
    w_out_attn,
    w_out_conv,
):
    whole = lax.all_gather(tokens, "tp", axis=1, tiled=True)
    rows_local = whole.shape[0]
    whole_float = whole.astype(jnp.float32)
    mean_square = jnp.mean(whole_float * whole_float, axis=1, keepdims=True)
    normed = (whole_float * lax.rsqrt(mean_square + norm_eps) * norm_gain).astype(jnp.bfloat16)
    col_widths = [
        w_query.shape[1],
        w_key.shape[1],
        w_value.shape[1],
        w_post_gate.shape[1],
        w_pre_gate.shape[1],
        w_conv_in.shape[1],
    ]
    joined = jnp.concatenate(
        (
            lax.all_gather(w_query, "sp", axis=0, tiled=True),
            lax.all_gather(w_key, "sp", axis=0, tiled=True),
            lax.all_gather(w_value, "sp", axis=0, tiled=True),
            lax.all_gather(w_post_gate, "sp", axis=0, tiled=True),
            lax.all_gather(w_pre_gate, "sp", axis=0, tiled=True),
            lax.all_gather(w_conv_in, "sp", axis=0, tiled=True),
        ),
        axis=1,
    )
    projected = jnp.dot(normed, joined, preferred_element_type=jnp.float32)
    bounds = []
    running = 0
    for col_width in col_widths[:-1]:
        running += col_width
        bounds.append(running)
    query_raw, key_raw, value_raw, post_gate, pre_gate, conv_input = jnp.split(
        projected, bounds, axis=1
    )
    offset = lax.axis_index("sp") * rows_local
    positions = offset + jnp.arange(rows_local, dtype=jnp.int32)
    local_heads = w_query.shape[1] // HEAD_DIM
    local_groups = w_key.shape[1] // HEAD_DIM
    group_size = local_heads // local_groups
    queries = axial_rotate(query_raw.reshape(rows_local, local_heads, HEAD_DIM), positions).astype(
        jnp.bfloat16
    )
    keys_rot = axial_rotate(key_raw.reshape(rows_local, local_groups, HEAD_DIM), positions).astype(
        jnp.bfloat16
    )
    key_value = jnp.concatenate(
        [keys_rot.reshape(rows_local, local_groups * HEAD_DIM), value_raw.astype(jnp.bfloat16)],
        axis=1,
    )
    mixed_input = (pre_gate * conv_input).astype(jnp.bfloat16)
    kv_padded = padded(key_value, (("sp", 0),), WINDOW)
    conv_padded = padded(mixed_input, (("sp", 0),), 1)
    conv_float = conv_padded.astype(jnp.float32)
    convolved = (
        conv_taps[0] * conv_float[:-2]
        + conv_taps[1] * conv_float[1:-1]
        + conv_taps[2] * conv_float[2:]
    )
    conv_out = (post_gate * convolved).astype(jnp.bfloat16)
    total_tokens = rows_local * lax.axis_size("sp")
    blocks = rows_local // WINDOW
    padded_rows = rows_local + 2 * WINDOW
    block_queries = queries.reshape(blocks, WINDOW, local_groups, group_size, HEAD_DIM)
    block_keys = block_windows(
        kv_padded[:, : local_groups * HEAD_DIM].reshape(padded_rows, local_groups, HEAD_DIM),
        rows_local,
        blocks,
    )
    block_values = block_windows(
        kv_padded[:, local_groups * HEAD_DIM :].reshape(padded_rows, local_groups, HEAD_DIM),
        rows_local,
        blocks,
    )
    scores = jnp.einsum(
        "nqkgd,nskd->nkgqs", block_queries, block_keys, preferred_element_type=jnp.float32
    ) * HEAD_DIM ** (-0.5)
    query_pos = positions.reshape(blocks, WINDOW)
    key_pos = (
        offset
        - WINDOW
        + (jnp.arange(blocks, dtype=jnp.int32) * WINDOW)[:, None]
        + jnp.arange(3 * WINDOW, dtype=jnp.int32)[None, :]
    )
    distance = key_pos[:, None, :] - query_pos[:, :, None]
    allowed = (
        (jnp.abs(distance) <= WINDOW)
        & (key_pos >= 0)[:, None, :]
        & (key_pos < total_tokens)[:, None, :]
    )
    scores = jnp.where(allowed[:, None, None], scores, -jnp.inf)
    sink_values = sink_logit.reshape(local_groups, group_size)[None, :, :, None]
    row_max = jnp.maximum(jnp.max(scores, axis=-1), sink_values)
    exp_scores = jnp.exp(scores - row_max[..., None])
    denominator = jnp.sum(exp_scores, axis=-1) + jnp.exp(sink_values - row_max)
    weights = (exp_scores / denominator[..., None]).astype(jnp.bfloat16)
    attended = (
        jnp.einsum("nkgqs,nskd->nqkgd", weights, block_values, preferred_element_type=jnp.float32)
        .astype(jnp.bfloat16)
        .reshape(rows_local, local_heads * HEAD_DIM)
    )
    log_sum = row_max + jnp.log(denominator)
    log_weight_sum = jnp.transpose(log_sum, (1, 2, 0, 3)).reshape(local_heads, rows_local)
    out_attn, out_conv = (
        lax.all_gather(w_out_attn, "sp", axis=1, tiled=True),
        lax.all_gather(w_out_conv, "sp", axis=1, tiled=True),
    )
    mixed = lax.psum_scatter(
        (
            jnp.dot(attended, out_attn, preferred_element_type=jnp.float32)
            + jnp.dot(conv_out, out_conv, preferred_element_type=jnp.float32)
        ).astype(jnp.bfloat16),
        "tp",
        scatter_dimension=0,
        tiled=True,
    )
    return (mixed, log_weight_sum)


def solution(mesh):
    placed = (
        P("sp", "tp"),
        P(),
        P("sp", "tp"),
        P("sp", "tp"),
        P("sp", "tp"),
        P("sp", "tp"),
        P("sp", "tp"),
        P("sp", "tp"),
        P(None, "tp"),
        P("tp"),
        P("tp", "sp"),
        P("tp", "sp"),
    )
    return jax.shard_map(
        on_device,
        mesh=mesh,
        in_specs=placed,
        out_specs=(P(("sp", "tp"), None), P("tp", "sp")),
        check_vma=False,
    )
```

profile of v0, /device:TPU:17, one launch (start us, length us, event | category | flops | bytes accessed | tf_op | source)
XLA Modules:
  0.0 324.2 jit_solution(14277394991578576114)
XLA Ops:
  11.2 0.7 all-gather.20.cloned.1.call-update
  12.1 0.9 copy.27
  13.0 22.1 %all_gather.29 = bf16[2048,64]{1,0:T(8,128)(2,1)S(1)} all-gather(bf16[256,64]{1,0:T(8,128)(2,1)S(1)} %copy.27), channel_id=1, replica_groups=mesh['sp'=8,'tp'=4] {'sp'}, dimensions={0}, use_global_device_ids=true | all-gather | bytes 294912 | tf_op jit(solution)/shard_map/all_gather | solution.py:92
  35.1 0.9 copy.28
  36.0 26.7 %all_gather.30 = bf16[2048,64]{1,0:T(8,128)(2,1)S(1)} all-gather(bf16[256,64]{1,0:T(8,128)(2,1)S(1)} %copy.28), channel_id=1, replica_groups=mesh['sp'=8,'tp'=4] {'sp'}, dimensions={0}, use_global_device_ids=true | all-gather | bytes 294912 | tf_op jit(solution)/shard_map/all_gather | solution.py:93
  62.6 1.4 fusion.91
  64.3 0.9 fusion.18
  65.3 27.8 %all-gather.12.cloned.1.call-done = bf16[2048,256]{1,0:T(8,128)(2,1)} async-done(((bf16[256,256]{1,0:T(8,128)(2,1)}), bf16[2048,256]{1,0:T(8,128)(2,1)}) %all-gather.12.cloned.1.call-update) | async-done | bytes 1048592 | tf_op jit(solution)/shard_map/all_gather | solution.py:94
  93.1 41.2 %all-gather.14.cloned.1.call-done = bf16[2048,256]{1,0:T(8,128)(2,1)} async-done(((bf16[256,256]{1,0:T(8,128)(2,1)}), bf16[2048,256]{1,0:T(8,128)(2,1)}) %all-gather.14.cloned.1.call-update) | async-done | bytes 1048592 | tf_op jit(solution)/shard_map/all_gather | solution.py:95
  134.3 41.0 %all-gather.16.cloned.1.call-done = bf16[2048,256]{1,0:T(8,128)(2,1)} async-done(((bf16[256,256]{1,0:T(8,128)(2,1)}), bf16[2048,256]{1,0:T(8,128)(2,1)}) %all-gather.16.cloned.1.call-update) | async-done | bytes 1048592 | tf_op jit(solution)/shard_map/all_gather | solution.py:96
  175.3 8.2 %concatenate.68 = bf16[2048,1152]{1,0:T(8,128)(2,1)} concatenate(bf16[2048,256]{1,0:T(8,128)(2,1)} %all-gather.10.cloned.1.call-done, bf16[2048,64]{1,0:T(8,128)(2,1)S(1)} %all_gather.29, bf16[2048,64]{1,0:T(8,128)(2,1)S(1)} %all_gather.30, bf16[2048,256]{1,0:T(8,128)(2,1)} %all-gather.12.cloned.1.call-done, bf16[2048,256]{1,0:T(8,128)(2,1)} %all-gather.14.cloned.1.call-done, ...), dimensions={1} | concatenate | bytes 9437184 | tf_op jit(solution)/shard_map/concatenate | solution.py:89
  183.5 17.4 %all-gather.8.cloned.1.call-done = bf16[512,2048]{1,0:T(8,128)(2,1)} async-done(((bf16[512,512]{1,0:T(8,128)(2,1)}), bf16[512,2048]{1,0:T(8,128)(2,1)}) %all-gather.8.cloned.1.call-update) | async-done | bytes 2097168 | tf_op jit(solution)/shard_map/all_gather | solution.py:76
  200.9 2.1 fusion
  202.9 5.9 %fusion.5 = f32[512,1152]{1,0:T(8,128)S(1)} fusion(bf16[2048,1152]{1,0:T(8,128)(2,1)} %concatenate.68, bf16[512,2048]{1,0:T(8,128)(2,1)} %all-gather.8.cloned.1.call-done, f32[2048]{0:T(1024)S(1)} %copy-done.7, f32[512]{0:T(512)S(1)} %add_rsqrt_fusion), kind=kOutput, calls=%fused_computation.11 | convolution fusion | flops 2420113408 | bytes 9185280 | tf_op jit(solution)/shard_map/dot_general | solution.py:100
  209.0 1.3 copy-done
  213.2 2.4 fusion.35
  215.9 3.1 collective-permute-start
  219.0 3.1 collective-permute-start.1
  222.1 2.2 collective-permute-start.3
  224.3 3.1 collective-permute-start.2
  230.2 0.9 maximum_convert_fusion
  231.1 0.8 fusion.70
  231.9 0.7 copy.37
  232.6 0.7 copy.36
  233.3 1.7 fusion.4
  235.0 1.6 copy.31
  236.7 0.7 copy.29
  238.3 0.9 fusion.14
  240.1 4.1 %fusion.41 = f32[512,2048]{1,0:T(8,128)} fusion(bf16[256,2048]{1,0:T(8,128)(2,1)} %all-gather.18.cloned.1.call-done, bf16[32,8,4,128]{3,2,1,0:T(4,128)(2,1)S(1)} %bitcast.108), kind=kOutput, calls=%fused_computation.51 | convolution fusion | flops 536870912 | bytes 5505024 | tf_op jit(solution)/shard_map/dot_general | solution.py:183
  244.2 36.5 %all-gather.20.cloned.1.call-done = bf16[256,2048]{1,0:T(8,128)(2,1)} async-done(((bf16[256,256]{1,0:T(8,128)(2,1)}), bf16[256,2048]{1,0:T(8,128)(2,1)}) %all-gather.20.cloned.1.call-update) | async-done | bytes 1048592 | tf_op jit(solution)/shard_map/all_gather | solution.py:179
  280.7 4.8 %add_convert_fusion = bf16[512,2048]{1,0:T(8,128)(2,1)} fusion(f32[512,2048]{1,0:T(8,128)} %fusion.41, bf16[256,2048]{1,0:T(8,128)(2,1)} %all-gather.20.cloned.1.call-done, f32[514,256]{1,0:T(8,128)S(1)} %copy-done.1, f32[512,1152]{1,0:T(8,128)} %copy-done, f32[256]{0:T(256)S(1)} %bitcast.127, f32[256]{0:T(256)S(1)} %bitcast.128, f32[256]{0:T(256)S(1)} %bitcast.126), kind=kOutput, calls=%fused_computation.5 | convolution fusion | flops 539885568 | bytes 9440256 | tf_op jit(solution)/shard_map/dot_general | solution.py:184
  286.2 31.1 %reduce-scatter.2.cloned.1.call-done = bf16[128,2048]{1,0:T(8,128)(2,1)} async-done(((bf16[512,2048]{1,0:T(8,128)(2,1)}), bf16[128,2048]{1,0:T(8,128)(2,1)}) %reduce-scatter.2.cloned.1.call-update) | async-done | bytes 524304 | tf_op jit(solution)/shard_map/reduce_scatter | solution.py:181
  (66 shorter events, 13.1 us)
Async XLA Ops:
  7.2 58.2 %all-gather.10.cloned.1.call-start = ((), (), s32[]{:S(2)}) async-start(), calls=%async_computation.2 | async-start | bytes 1179648 | tf_op jit(solution)/shard_map/all_gather | solution.py:91
  7.9 85.2 %all-gather.12.cloned.1.call-start = ((), (), s32[]{:S(2)}) async-start(), calls=%async_computation.3 | async-start | bytes 1179648 | tf_op jit(solution)/shard_map/all_gather | solution.py:94
  8.6 125.6 %all-gather.14.cloned.1.call-start = ((), (), s32[]{:S(2)}) async-start(), calls=%async_computation.4 | async-start | bytes 1179648 | tf_op jit(solution)/shard_map/all_gather | solution.py:95
  9.4 165.9 %all-gather.16.cloned.1.call-start = ((), (), s32[]{:S(2)}) async-start(), calls=%async_computation.5 | async-start | bytes 1179648 | tf_op jit(solution)/shard_map/all_gather | solution.py:96
  10.0 190.9 %all-gather.8.cloned.1.call-start = ((), (), s32[]{:S(2)}) async-start(), calls=%async_computation.1 | async-start | bytes 2621440 | tf_op jit(solution)/shard_map/all_gather | solution.py:76
  10.5 229.6 %all-gather.18.cloned.1.call-start = ((), (), s32[]{:S(2)}) async-start(), calls=%async_computation.6 | async-start | bytes 1179648 | tf_op jit(solution)/shard_map/all_gather | solution.py:178
  11.1 269.5 %all-gather.20.cloned.1.call-start = ((), (), s32[]{:S(2)}) async-start(), calls=%async_computation.7 | async-start | bytes 1179648 | tf_op jit(solution)/shard_map/all_gather | solution.py:179
  11.9 305.5 %reduce-scatter.2.cloned.1.call-start = ((), (), s32[]{:S(2)}) async-start(), calls=%async_computation.8 | async-start | bytes 2621440 | tf_op jit(solution)/shard_map/reduce_scatter | solution.py:181
  65.3 137.6 %copy-start.7 = (f32[2048]{0:T(1024)S(1)}, f32[2048]{0:T(1024)}, u32[]{:S(2)}) copy-start(f32[2048]{0:T(1024)} %param.13) | copy-start | bytes 24580
  208.8 1.4 copy-start
  215.9 15.2 %collective-permute-start = (bf16[128,128]{1,0:T(8,128)(2,1)S(1)}, bf16[128,128]{1,0:T(8,128)(2,1)S(1)}, u32[]{:S(2)}, u32[]{:S(2)}) collective-permute-start(bf16[128,128]{1,0:T(8,128)(2,1)S(1)} %get-tuple-element.24), channel_id=1, source_target_pairs={{0,4},{4,8},{8,12},{12,16},{16,20},{20,24},{24,28},{1,5},{5,9},{9,... | collective-permute-start | bytes 98312 | tf_op jit(solution)/shard_map/ppermute | solution.py:20
  219.0 12.1 %collective-permute-start.1 = (bf16[128,128]{1,0:T(8,128)(2,1)S(1)}, bf16[128,128]{1,0:T(8,128)(2,1)S(1)}, u32[]{:S(2)}, u32[]{:S(2)}) collective-permute-start(bf16[128,128]{1,0:T(8,128)(2,1)S(1)} %get-tuple-element.25), channel_id=1, source_target_pairs={{4,0},{8,4},{12,8},{16,12},{20,16},{24,20},{28,24},{5,1},{9,5},{13... | collective-permute-start | bytes 98312 | tf_op jit(solution)/shard_map/ppermute | solution.py:23
  222.1 8.1 %collective-permute-start.3 = (bf16[1,256]{1,0:T(2,128)(2,1)S(1)}, bf16[1,256]{1,0:T(2,128)(2,1)S(1)}, u32[]{:S(2)}, u32[]{:S(2)}) collective-permute-start(bf16[1,256]{1,0:T(2,128)(2,1)S(1)} %get-tuple-element.17), channel_id=1, source_target_pairs={{4,0},{8,4},{12,8},{16,12},{20,16},{24,20},{28,24},{5,1},{9,5},{13... | collective-permute-start | bytes 1544 | tf_op jit(solution)/shard_map/ppermute | solution.py:23
  224.3 6.0 %collective-permute-start.2 = (bf16[1,256]{1,0:T(2,128)(2,1)S(1)}, bf16[1,256]{1,0:T(2,128)(2,1)S(1)}, u32[]{:S(2)}, u32[]{:S(2)}) collective-permute-start(bf16[1,256]{1,0:T(2,128)(2,1)S(1)} %get-tuple-element.16), channel_id=1, source_target_pairs={{0,4},{4,8},{8,12},{12,16},{16,20},{20,24},{24,28},{1,5},{5,9},{9,... | collective-permute-start | bytes 1544 | tf_op jit(solution)/shard_map/ppermute | solution.py:20
  231.9 5.5 %copy-start.4 = (f32[4]{0:T(128)S(1)}, f32[4]{0:T(128)}, u32[]{:S(2)}) copy-start(f32[4]{0:T(128)} %param.21) | copy-start | bytes 52
  237.4 0.8 copy-start.2
  237.4 0.9 copy-start.3
  240.1 40.5 %copy-start.1 = (f32[514,256]{1,0:T(8,128)S(1)}, f32[514,256]{1,0:T(8,128)}, u32[]{:S(2)}) copy-start(f32[514,256]{1,0:T(8,128)} %maximum_convert_fusion) | copy-start | bytes 1579012
  240.1 40.5 %copy-start.5 = (f32[1,256]{1,0:T(1,128)S(1)}, f32[1,256]{1,0:T(1,128)}, u32[]{:S(2)}) copy-start(f32[1,256]{1,0:T(1,128)} %get-tuple-element.27) | copy-start | bytes 3076
  240.1 40.5 %copy-start.6 = (f32[1,256]{1,0:T(1,128)S(1)}, f32[1,256]{1,0:T(1,128)}, u32[]{:S(2)}) copy-start(f32[1,256]{1,0:T(1,128)} %get-tuple-element.28) | copy-start | bytes 3076
Sparse Core Ops, SparseCore 0:
  10.1 41.4 all-gather.9
  53.8 39.3 all-gather.11
  95.3 38.9 all-gather.13
  136.3 38.9 all-gather.15
  176.7 24.1 all-gather.7
  202.8 37.3 all-gather.17
  242.2 38.4 all-gather.19
  285.6 31.6 reduce-scatter.1
where the time goes:
time: 327 us; the launch traced here: 324 us
  waiting for transfers between devices  200 us (61%)
  blocking collectives  48.8 us (15%)
  local copies, waits for them, and re-layouts  22.6 us (7%)
  matrix products  17.4 us (5%)
  between operations  14.4 us (4%)
  starting transfers between devices  11.8 us (4%)
  other arithmetic  9.22 us (3%)
    all_gather x1, waiting for transfers between devices, on_device(): lax.all_gather(w_pre_gate, 'sp', axis=0, tiled=True)  41.2 us
    all_gather x1, waiting for transfers between devices, on_device(): lax.all_gather(w_conv_in, 'sp', axis=0, tiled=True)  41 us
    all_gather x1, waiting for transfers between devices, on_device(): lax.all_gather(w_out_conv, 'sp', axis=1, tiled=True)  36.5 us
    reduce_scatter x1, waiting for transfers between devices, on_device(): lax.psum_scatter((jnp.dot(attended, out_attn, preferred_element_type=jnp....  31.1 us
    all_gather x1, waiting for transfers between devices, on_device(): lax.all_gather(w_post_gate, 'sp', axis=0, tiled=True)  27.8 us
    all_gather x1, blocking collectives, on_device(): lax.all_gather(w_value, 'sp', axis=0, tiled=True)  26.7 us
    all_gather x1, blocking collectives, on_device(): lax.all_gather(w_key, 'sp', axis=0, tiled=True)  22.1 us
    all_gather x1, waiting for transfers between devices, on_device(): whole = lax.all_gather(tokens, 'tp', axis=1, tiled=True)  17.4 us
  transfers between devices with their start and end apart: 12, of which 7 were waited for; matrix products, arithmetic and copies ran while one was open for 13% of the time, Pallas kernels for 0%

commit v1 on v0

--- a/solution.py
+++ b/solution.py
@@ -1,7 +1,13 @@
+import functools
+
 import jax
 import jax.numpy as jnp
 from jax import lax
+from jax.experimental import pallas as pl
+from jax.experimental.pallas import tpu as pltpu
 from jax.sharding import PartitionSpec as P
+
+MESH = pl.DeviceIdType.MESH
 
 HEAD_DIM = 64
 WINDOW = 128
@@ -190,6 +196,536 @@
     return (mixed, log_weight_sum)
 
 
+def rope_tables(rows, lanes):
+    half_dim = HEAD_DIM // 2
+    positions = lax.axis_index("sp") * rows + jnp.arange(rows, dtype=jnp.int32)
+    lane = jnp.arange(lanes, dtype=jnp.int32) % HEAD_DIM
+    freq_index = lane % (half_dim // 2)
+    inv_freq = rope_base ** (-(2 * freq_index).astype(jnp.float32) / half_dim)
+    is_col = lane >= half_dim
+    index = jnp.where(is_col[None, :], (positions % GRID_W)[:, None], (positions // GRID_W)[:, None])
+    angle = index.astype(jnp.float32) * inv_freq[None, :]
+    sign = jnp.where((lane % half_dim) < half_dim // 2, -1.0, 1.0)
+    return jnp.cos(angle), jnp.sin(angle) * sign[None, :]
+
+
+def fused_kernel(
+    Z, X,
+    tok_ref, gain_ref, win_ref, oa_ref, oc_ref, cos_ref, sin_ref, taps_ref, sink_ref,
+    out_ref, lse_ref,
+    tok, normed, win, woa, woc, acc, qbuf, kvp, cf, chalo_out, chalo_in, att, cout,
+    part_keep, part_send, part_recv, y_send, y_recv,
+    tok_sem, in_send, in_recv, oa_send, oa_recv, oc_send, oc_recv, halo_sem, rs_sem, loc_sem,
+):
+    S = Z * X
+    rows, width = tok_ref.shape
+    depth = win_ref.shape[0]
+    cols = oa_ref.shape[1]
+    qw = qbuf.shape[1]
+    cw = cf.shape[1]
+    sp = lax.axis_index("sp")
+    tp = lax.axis_index("tp")
+    z, x = sp // X, sp % X
+    core, yy = tp % 2, tp // 2
+    sib = tp + 1 - 2 * core
+    ynb = (1 - yy) * 2 + core
+    ysib = (1 - yy) * 2 + 1 - core
+    xnb = z * X + 1 - x
+    low, high = sp - X, sp + X
+    has_low, has_high = z > 0, z < Z - 1
+    has_prev, has_next = sp > 0, sp < S - 1
+
+    barrier = pltpu.get_barrier_semaphore()
+
+    def greet(dev):
+        pl.semaphore_signal(barrier, inc=1, device_id=dev, device_id_type=MESH)
+
+    greet((xnb, tp))
+    greet((sp, sib))
+    greet((sp, ynb))
+    for cond, dev in ((has_low, low), (has_high, high), (has_prev, sp - 1), (has_next, sp + 1)):
+        @pl.when(cond)
+        def _(dev=dev):
+            greet((dev, tp))
+    peers = 3
+    for cond in (has_low, has_high, has_prev, has_next):
+        peers = peers + jnp.where(cond, 1, 0)
+    pl.semaphore_wait(barrier, peers)
+
+    def remote(src, dst, ssem, rsem, dev):
+        return pltpu.make_async_remote_copy(
+            src_ref=src, dst_ref=dst, send_sem=ssem, recv_sem=rsem,
+            device_id=dev, device_id_type=MESH,
+        )
+
+    targets = (low, high, xnb)
+
+    def weight_copy(kind, slot, direction, own=False):
+        buf, ssem, rsem, ref = (
+            (win, in_send, in_recv, win_ref),
+            (woa, oa_send, oa_recv, oa_ref),
+            (woc, oc_send, oc_recv, oc_ref),
+        )[kind]
+        source = ref if own else buf.at[slot]
+        return remote(source, buf.at[slot], ssem.at[direction, slot], rsem.at[slot], (targets[direction], tp))
+
+    weight_copy(2, sp, 2, True).start()
+    @pl.when(has_low)
+    def _():
+        weight_copy(0, sp, 0, True).start()
+    @pl.when(has_high)
+    def _():
+        weight_copy(0, sp, 1, True).start()
+    weight_copy(0, sp, 2, True).start()
+
+    tok_y = remote(tok_ref, tok.at[tp], tok_sem.at[0], tok_sem.at[1], (sp, ynb))
+    tok_y.start()
+    tok_s = remote(tok_ref, tok.at[tp], tok_sem.at[2], tok_sem.at[3], (sp, sib))
+    tok_s.start()
+    local = [
+        pltpu.make_async_copy(tok_ref, tok.at[tp], loc_sem.at[0]),
+        pltpu.make_async_copy(win_ref, win.at[sp], loc_sem.at[1]),
+        pltpu.make_async_copy(oa_ref, woa.at[sp], loc_sem.at[2]),
+        pltpu.make_async_copy(oc_ref, woc.at[sp], loc_sem.at[3]),
+    ]
+    for copy in local:
+        copy.start()
+    for copy in local:
+        copy.wait()
+    remote(tok.at[ynb], tok.at[ynb], tok_sem.at[0], tok_sem.at[1], (sp, ynb)).wait_recv()
+    tok_f = remote(tok.at[ynb], tok.at[ynb], tok_sem.at[4], tok_sem.at[5], (sp, sib))
+    tok_f.start()
+    remote(tok.at[sib], tok.at[sib], tok_sem.at[2], tok_sem.at[3], (sp, sib)).wait_recv()
+    remote(tok.at[ysib], tok.at[ysib], tok_sem.at[4], tok_sem.at[5], (sp, sib)).wait_recv()
+
+    TP = tok.shape[0]
+    RB = 64
+
+    def norm_rows(i, carry):
+        r = pl.ds(pl.multiple_of(i * RB, RB), RB)
+        total = jnp.zeros((RB, 1), jnp.float32)
+        for t in range(TP):
+            v = tok[t, r, :].astype(jnp.float32)
+            total += jnp.sum(v * v, axis=1, keepdims=True)
+        scale = lax.rsqrt(total / (TP * width) + norm_eps)
+        for t in range(TP):
+            v = tok[t, r, :].astype(jnp.float32)
+            g = gain_ref[:, t * width:(t + 1) * width]
+            normed[r, t * width:(t + 1) * width] = (v * scale * g).astype(jnp.bfloat16)
+        return carry
+
+    lax.fori_loop(0, rows // RB, norm_rows, 0)
+
+    MB = 128
+
+    def project(slot, first):
+        def body(i, carry):
+            r = pl.ds(pl.multiple_of(i * MB, MB), MB)
+            c = pl.ds(pl.multiple_of(slot * depth, depth), depth)
+            prod = jnp.dot(normed[r, c], win[slot], preferred_element_type=jnp.float32)
+            if first:
+                acc[r, :] = prod
+            else:
+                acc[r, :] += prod
+            return carry
+        lax.fori_loop(0, rows // MB, body, 0)
+
+    def entry(k):
+        dist = (k + 1) // 2
+        up = 1 - k % 2
+        zz = z + dist * (2 * up - 1)
+        return zz, up, (zz >= 0) & (zz < Z)
+
+    def wait_weight(kind, slot):
+        weight_copy(kind, slot, 2).wait_recv()
+
+    def pass_on(kind, slot, up, across):
+        @pl.when((up == 1) & has_low)
+        def _():
+            weight_copy(kind, slot, 0).start()
+        @pl.when((up == 0) & has_high)
+        def _():
+            weight_copy(kind, slot, 1).start()
+        if across:
+            weight_copy(kind, slot, 2).start()
+
+    entries = 2 * Z - 1
+
+    def start_out_weights():
+        for direction, cond in ((0, has_low), (1, has_high)):
+            @pl.when(cond)
+            def _(direction=direction):
+                weight_copy(1, sp, direction, True).start()
+                weight_copy(2, sp, direction, True).start()
+        weight_copy(1, sp, 2, True).start()
+        wait_weight(2, xnb)
+        for direction, cond in ((0, has_low), (1, has_high)):
+            @pl.when(cond)
+            def _(direction=direction):
+                weight_copy(2, xnb, direction).start()
+
+    project(sp, True)
+
+    def in_step(k, carry):
+        zz, up, valid = entry(k)
+
+        @pl.when(valid & (k < entries))
+        def _():
+            slot = zz * X + x
+            wait_weight(0, slot)
+            pass_on(0, slot, up, True)
+            project(slot, False)
+
+        @pl.when(k == 2 * (Z - 2))
+        def _():
+            start_out_weights()
+
+        zo, _, valid_o = entry(k - 2)
+
+        @pl.when(valid_o & (k >= 2))
+        def _():
+            slot = zo * X + 1 - x
+            wait_weight(0, slot)
+            project(slot, False)
+        return carry
+
+    lax.fori_loop(1, entries + 2, in_step, 0)
+
+    def out_comm(dist):
+        for up in (0, 1):
+            zz = z + dist * (2 * up - 1)
+
+            @pl.when((zz >= 0) & (zz < Z))
+            def _(zz=zz, up=up):
+                mine, other = zz * X + x, zz * X + 1 - x
+                wait_weight(1, mine)
+                pass_on(1, mine, up, True)
+                wait_weight(2, mine)
+                pass_on(2, mine, up, False)
+                wait_weight(2, other)
+                pass_on(2, other, up, False)
+
+    def turned(v, cosv, sinv):
+        lane = lax.broadcasted_iota(jnp.int32, v.shape, 1)
+        quarter = HEAD_DIM // 4
+        partner = jnp.where(
+            lane % (2 * quarter) < quarter,
+            pltpu.roll(v, v.shape[1] - quarter, 1),
+            pltpu.roll(v, quarter, 1),
+        )
+        return v * cosv + partner * sinv
+
+    kw = 2 * HEAD_DIM
+
+    def kv_rows(i, carry):
+        r = pl.ds(pl.multiple_of(i * MB, MB), MB)
+        v = acc[r, qw:qw + kw]
+        lane = lax.broadcasted_iota(jnp.int32, v.shape, 1)
+        kv = jnp.where(lane < HEAD_DIM, turned(v, cos_ref[r, :], sin_ref[r, :]), v)
+        kvp[pl.ds(pl.multiple_of(WINDOW + i * MB, MB), MB), :] = kv.astype(jnp.bfloat16)
+        base = qw + kw + cw
+        mi = (acc[r, base:base + cw] * acc[r, base + cw:base + 2 * cw]).astype(jnp.bfloat16)
+        cf[pl.ds(pl.multiple_of(8 + i * MB, 8), MB), :] = mi.astype(jnp.float32)
+        return carry
+
+    lax.fori_loop(0, rows // MB, kv_rows, 0)
+    E = chalo_out.shape[1]
+    chalo_out[0] = cf[8:8 + E, :].astype(jnp.bfloat16)
+    chalo_out[1] = cf[8 + rows - E:8 + rows, :].astype(jnp.bfloat16)
+
+    to_next = [
+        remote(kvp.at[pl.ds(rows, WINDOW)], kvp.at[pl.ds(0, WINDOW)], halo_sem.at[0], halo_sem.at[1], (sp + 1, tp)),
+        remote(chalo_out.at[1], chalo_in.at[0], halo_sem.at[2], halo_sem.at[3], (sp + 1, tp)),
+    ]
+    to_prev = [
+        remote(kvp.at[pl.ds(WINDOW, WINDOW)], kvp.at[pl.ds(WINDOW + rows, WINDOW)], halo_sem.at[4], halo_sem.at[5], (sp - 1, tp)),
+        remote(chalo_out.at[0], chalo_in.at[1], halo_sem.at[6], halo_sem.at[7], (sp - 1, tp)),
+    ]
+
+    @pl.when(has_next)
+    def _():
+        for copy in to_next:
+            copy.start()
+
+    @pl.when(has_prev)
+    def _():
+        for copy in to_prev:
+            copy.start()
+
+    out_comm(1)
+
+    def q_rows(i, carry):
+        r = pl.ds(pl.multiple_of(i * MB, MB), MB)
+        for c in range(qw // kw):
+            qbuf[r, c * kw:(c + 1) * kw] = turned(
+                acc[r, c * kw:(c + 1) * kw], cos_ref[r, :], sin_ref[r, :]
+            ).astype(jnp.bfloat16)
+        return carry
+
+    lax.fori_loop(0, rows // MB, q_rows, 0)
+
+    zero_kv = jnp.zeros((WINDOW, kw), jnp.bfloat16)
+    zero_c = jnp.zeros((8, cw), jnp.float32)
+
+    @pl.when(has_prev)
+    def _():
+        for copy in to_next:
+            copy.wait_recv()
+        cf[0:8, :] = chalo_in[0, E - 8:E, :].astype(jnp.float32)
+
+    @pl.when(jnp.logical_not(has_prev))
+    def _():
+        kvp[0:WINDOW, :] = zero_kv
+        cf[0:8, :] = zero_c
+
+    @pl.when(has_next)
+    def _():
+        for copy in to_prev:
+            copy.wait_recv()
+        cf[8 + rows:16 + rows, :] = chalo_in[1, 0:8, :].astype(jnp.float32)
+
+    @pl.when(jnp.logical_not(has_next))
+    def _():
+        kvp[WINDOW + rows:, :] = zero_kv
+        cf[8 + rows:16 + rows, :] = zero_c
+
+    taps = [taps_ref[t:t + 1, :] for t in range(3)]
+    for i in range(rows // MB):
+        a = 8 + i * MB
+        conv = (
+            taps[0] * cf[a - 1:a - 1 + MB, :]
+            + taps[1] * cf[a:a + MB, :]
+            + taps[2] * cf[a + 1:a + 1 + MB, :]
+        )
+        cout[i * MB:(i + 1) * MB, :] = (acc[i * MB:(i + 1) * MB, qw + kw:qw + kw + cw] * conv).astype(jnp.bfloat16)
+
+    heads = qw // HEAD_DIM
+    K3 = 3 * WINDOW
+    total_tokens = rows * S
+
+    def attend(b, carry):
+        r = pl.ds(pl.multiple_of(b * WINDOW, WINDOW), WINDOW)
+        kv = kvp[pl.ds(pl.multiple_of(b * WINDOW, WINDOW), K3), :].astype(jnp.float32)
+        lane = lax.broadcasted_iota(jnp.int32, (K3, kw), 1)
+        swapped = pltpu.roll(kv, HEAD_DIM, 1)
+        kk = jnp.where(lane < HEAD_DIM, kv, swapped).astype(jnp.bfloat16)
+        vv = jnp.where(lane < HEAD_DIM, swapped, kv).astype(jnp.bfloat16)
+        k_half = [jnp.where(lane < HEAD_DIM, kk, 0), jnp.where(lane < HEAD_DIM, 0, kk)]
+        v_half = [jnp.where(lane < HEAD_DIM, vv, 0), jnp.where(lane < HEAD_DIM, 0, vv)]
+        qi = lax.broadcasted_iota(jnp.int32, (WINDOW, K3), 0)
+        ki = lax.broadcasted_iota(jnp.int32, (WINDOW, K3), 1)
+        first = sp * rows + b * WINDOW - WINDOW
+        allowed = (ki >= qi) & (ki <= qi + 2 * WINDOW) & (ki + first >= 0) & (ki + first < total_tokens)
+        lse_lane = lax.broadcasted_iota(jnp.int32, (WINDOW, WINDOW), 1)
+        lse_all = jnp.zeros((WINDOW, WINDOW), jnp.float32)
+        for pair in range(heads // 2):
+            q = qbuf[r, pair * kw:(pair + 1) * kw]
+            total = jnp.zeros((WINDOW, kw), jnp.float32)
+            for side in range(2):
+                h = pair * 2 + side
+                s = lax.dot_general(
+                    q, k_half[side], (((1,), (1,)), ((), ())), preferred_element_type=jnp.float32
+                ) * HEAD_DIM ** (-0.5)
+                s = jnp.where(allowed, s, -jnp.inf)
+                sink = sink_ref[h:h + 1, 0:1]
+                top = jnp.maximum(jnp.max(s, axis=1, keepdims=True), sink)
+                e = jnp.exp(s - top)
+                den = jnp.sum(e, axis=1, keepdims=True) + jnp.exp(sink - top)
+                w = (e * (1.0 / den)).astype(jnp.bfloat16)
+                total += jnp.dot(w, v_half[side], preferred_element_type=jnp.float32)
+                lse_all = jnp.where(lse_lane == h, top + jnp.log(den), lse_all)
+            att[r, pair * kw:(pair + 1) * kw] = total.astype(jnp.bfloat16)
+        lse_ref[:, r] = jnp.transpose(lse_all)[0:heads, :]
+        return carry
+
+    blocks = rows // WINDOW
+    lax.fori_loop(0, blocks // 2, attend, 0)
+    if Z > 2:
+        out_comm(2)
+    lax.fori_loop(blocks // 2, blocks, attend, 0)
+    for dist in range(3, Z):
+        out_comm(dist)
+
+    chunk = rows // TP
+
+    def sib_copy(slot):
+        return remote(part_send.at[slot], part_recv.at[slot], rs_sem.at[0, slot], rs_sem.at[1, slot], (sp, sib))
+
+    def y_copy(slot):
+        return remote(y_send.at[slot], y_recv.at[slot], rs_sem.at[2, slot], rs_sem.at[3, slot], (sp, ynb))
+
+    def out_block(slot):
+        for half in range(2):
+            for mine in range(2):
+                t = half * 2 + (core if mine else 1 - core)
+                r = pl.ds(pl.multiple_of(t * chunk, chunk), chunk)
+                v = jnp.dot(att[r, :], woa[slot], preferred_element_type=jnp.float32) + jnp.dot(
+                    cout[r, :], woc[slot], preferred_element_type=jnp.float32
+                )
+                if mine:
+                    part_keep[slot, half] = v
+                else:
+                    part_send[slot, half] = v.astype(jnp.bfloat16)
+        sib_copy(slot).start()
+
+    def y_block(slot):
+        sib_copy(slot).wait_recv()
+        y_send[slot] = (
+            part_keep[slot, 1 - yy] + part_recv[slot, 1 - yy].astype(jnp.float32)
+        ).astype(jnp.bfloat16)
+        y_copy(slot).start()
+
+    def finish(slot):
+        y_copy(slot).wait_recv()
+        out_ref[:, pl.ds(pl.multiple_of(slot * cols, cols), cols)] = (
+            part_keep[slot, yy]
+            + part_recv[slot, yy].astype(jnp.float32)
+            + y_recv[slot].astype(jnp.float32)
+        ).astype(jnp.bfloat16)
+
+    def each(fn, lo, hi):
+        def step(u, carry):
+            k, side = u // 2, u % 2
+            zz, _, valid = entry(k)
+
+            @pl.when(valid)
+            def _():
+                slot = zz * X + jnp.where(side == 0, x, 1 - x)
+                fn(slot, k, side)
+            return carry
+        lax.fori_loop(lo, hi, step, 0)
+
+    def project_out(slot, k, side):
+        @pl.when(side == 1)
+        def _():
+            wait_weight(1, slot)
+        out_block(slot)
+
+    half_u = entries
+    each(project_out, 0, half_u)
+    each(lambda slot, k, side: y_block(slot), 0, half_u)
+    each(project_out, half_u, 2 * entries)
+    each(lambda slot, k, side: y_block(slot), half_u, 2 * entries)
+    each(lambda slot, k, side: finish(slot), 0, 2 * entries)
+
+    tok_y.wait_send()
+    tok_s.wait_send()
+    tok_f.wait_send()
+
+    @pl.when(has_next)
+    def _():
+        for copy in to_next:
+            copy.wait_send()
+
+    @pl.when(has_prev)
+    def _():
+        for copy in to_prev:
+            copy.wait_send()
+
+    def drain(zz, carry):
+        mine, other = zz * X + x, zz * X + 1 - x
+        for direction, cond in ((0, (zz >= z) & has_low), (1, (zz <= z) & has_high)):
+            @pl.when(cond)
+            def _(direction=direction):
+                weight_copy(0, mine, direction).wait_send()
+                weight_copy(1, mine, direction).wait_send()
+                weight_copy(2, mine, direction).wait_send()
+                weight_copy(2, other, direction).wait_send()
+        weight_copy(0, mine, 2).wait_send()
+        weight_copy(1, mine, 2).wait_send()
+        for slot in (mine, other):
+            sib_copy(slot).wait_send()
+            y_copy(slot).wait_send()
+        return carry
+
+    lax.fori_loop(0, Z, drain, 0)
+    weight_copy(2, sp, 2).wait_send()
+
+
+def fused(
+    tokens, norm_gain, w_query, w_key, w_value, w_post_gate, w_pre_gate, w_conv_in,
+    conv_taps, sink_logit, w_out_attn, w_out_conv,
+):
+    S, TP = lax.axis_size("sp"), lax.axis_size("tp")
+    X = 2
+    Z = S // X
+    rows, width = tokens.shape
+    depth, qw = w_query.shape
+    cw = w_post_gate.shape[1]
+    cols = w_out_attn.shape[1]
+    heads = qw // HEAD_DIM
+    kw = 2 * HEAD_DIM
+    joined = jnp.concatenate((w_query, w_key, w_value, w_post_gate, w_pre_gate, w_conv_in), axis=1)
+    nw = joined.shape[1]
+    cosv, sinv = rope_tables(rows, kw)
+    chunk = rows // TP
+    bf, f32 = jnp.bfloat16, jnp.float32
+    dma = pltpu.SemaphoreType.DMA
+    sinks = jnp.broadcast_to(sink_logit[:, None], (heads, kw))
+    return pl.pallas_call(
+        functools.partial(fused_kernel, Z, X),
+        out_shape=(
+            jax.ShapeDtypeStruct((chunk, S * cols), bf),
+            jax.ShapeDtypeStruct((heads, rows), f32),
+        ),
+        in_specs=[pl.BlockSpec(memory_space=pltpu.VMEM)] * 9,
+        out_specs=(pl.BlockSpec(memory_space=pltpu.VMEM),) * 2,
+        scratch_shapes=[
+            pltpu.VMEM((TP, rows, width), bf),
+            pltpu.VMEM((rows, TP * width), bf),
+            pltpu.VMEM((S, depth, nw), bf),
+            pltpu.VMEM((S,) + w_out_attn.shape, bf),
+            pltpu.VMEM((S,) + w_out_conv.shape, bf),
+            pltpu.VMEM((rows, nw), f32),
+            pltpu.VMEM((rows, qw), bf),
+            pltpu.VMEM((rows + 2 * WINDOW, kw), bf),
+            pltpu.VMEM((rows + 16, cw), f32),
+            pltpu.VMEM((2, 16, cw), bf),
+            pltpu.VMEM((2, 16, cw), bf),
+            pltpu.VMEM((rows, qw), bf),
+            pltpu.VMEM((rows, cw), bf),
+            pltpu.VMEM((S, 2, chunk, cols), f32),
+            pltpu.VMEM((S, 2, chunk, cols), bf),
+            pltpu.VMEM((S, 2, chunk, cols), bf),
+            pltpu.VMEM((S, chunk, cols), bf),
+            pltpu.VMEM((S, chunk, cols), bf),
+            dma((6,)),
+            dma((3, S)), dma((S,)),
+            dma((3, S)), dma((S,)),
+            dma((3, S)), dma((S,)),
+            dma((8,)),
+            dma((4, S)),
+            dma((4,)),
+        ],
+        compiler_params=pltpu.CompilerParams(
+            collective_id=0, has_side_effects=True, vmem_limit_bytes=60 * 1024 * 1024
+        ),
+    )(tokens, norm_gain[None, :], joined, w_out_attn, w_out_conv, cosv, sinv, conv_taps, sinks)
+
+
+def fits(
+    tokens, norm_gain, w_query, w_key, w_value, w_post_gate, w_pre_gate, w_conv_in,
+    conv_taps, sink_logit, w_out_attn, w_out_conv,
+):
+    S, TP = lax.axis_size("sp"), lax.axis_size("tp")
+    return (
+        TP == 4
+        and S % 2 == 0
+        and S >= 4
+        and w_key.shape[1] == HEAD_DIM
+        and w_query.shape[0] % 128 == 0
+        and w_query.shape[1] % 128 == 0
+        and w_post_gate.shape[1] % 128 == 0
+        and w_out_attn.shape[1] % 128 == 0
+        and tokens.shape[0] % (TP * WINDOW) == 0
+        and tokens.shape[1] % 128 == 0
+    )
+
+
+def either(*args):
+    return fused(*args) if fits(*args) else on_device(*args)
+
+
 def solution(mesh):
     placed = (
         P("sp", "tp"),
@@ -206,7 +742,7 @@
         P("tp", "sp"),
     )
     return jax.shard_map(
-        on_device,
+        either,
         mesh=mesh,
         in_specs=placed,
         out_specs=(P(("sp", "tp"), None), P("tp", "sp")),

time: 327 us -> 113 us (0.35)
  the two profiles are of different devices: /device:TPU:17 before, /device:TPU:0 now
where the time goes in v1:
time: 113 us; the launch traced here: 112 us
  Pallas kernels  102 us (90%)
  local copies, waits for them, and re-layouts  7.4 us (7%)
  other arithmetic  1.85 us (2%)
    pallas_call x1, Pallas kernels, fused(): pl.pallas_call(functools.partial(fused_kernel, Z, X), out_shape=(jax.Shap...  102 us
    unnamed x8, local copies, waits for them, and re-layouts  4.24 us

profile of v1, /device:TPU:0, one launch (start us, length us, event | category | flops | bytes accessed | tf_op | source)
XLA Modules:
  0.0 112.1 jit_solution(17718503736798277802)
XLA Ops:
  0.6 0.0 copy-start
  0.7 1.3 %broadcast_in_dim.52.sink_ref = f32[4,128]{1,0:T(4,128)} broadcast(f32[4]{0:T(128)} %param.21), dimensions={0} | broadcast | bytes 2064 | tf_op jit(solution)/shard_map/broadcast_in_dim | solution.py:664
  2.0 0.9 copy.14
  2.9 0.9 copy.15
  3.8 0.0 copy-done
  3.8 1.8 %concatenate.3.win_ref = bf16[256,1152]{1,0:T(8,128)(2,1)} concatenate(bf16[256,256]{1,0:T(8,128)(2,1)S(1)} %copy-done, bf16[256,64]{1,0:T(8,128)(2,1)S(1)} %copy.14, bf16[256,64]{1,0:T(8,128)(2,1)S(1)} %copy.15, bf16[256,256]{1,0:T(8,128)(2,1)} %param.17, bf16[256,256]{1,0:T(8,128)(2,1)} %param.18, bf16[256,256]{1,0:T(8,128)(2,1)} %param.19), dimensions={1} | concatenate | bytes 1179648 | tf_op jit(solution)/shard_map/concatenate | solution.py:658
  5.6 1.8 %sine_multiply_fusion = (f32[512,128]{1,0:T(8,128)}, f32[512,128]{1,0:T(8,128)}) fusion(f32[128]{0:T(128)S(1)} %get-tuple-element.6, f32[128]{0:T(128)S(1)} %get-tuple-element.7, s32[512]{0:T(512)S(1)} %get-tuple-element.4, s32[512]{0:T(512)S(1)} %get-tuple-element.5, pred[128]{0:T(512)(128)(4,1)S(1)} %broadcast_compare_fusion), kind=kLoop, calls=%fused_computation | loop fusion | flops 262144 | bytes 529536 | tf_op jit(solution)/shard_map/mul | solution.py:209
  7.4 102.2 %shard_map.131 = (bf16[128,2048]{1,0:T(8,128)(2,1)}, f32[4,512]{1,0:T(4,128)}) custom-call(bf16[512,512]{1,0:T(8,128)(2,1)} %tok_ref.1, f32[1,2048]{1,0:T(1,128)} %bitcast.1, bf16[256,1152]{1,0:T(8,128)(2,1)} %concatenate.3.win_ref, bf16[256,256]{1,0:T(8,128)(2,1)} %oa_ref.1, bf16[256,256]{1,0:T(8,128)(2,1)} %oc_ref.1, f32[512,128]{1,0:T(8,128)} %get-tuple-element.3.cos_ref, ...), custom_call_target="tpu_custom_call" | custom-call | tf_op jit(solution)/shard_map/pallas_call | solution.py:665
  109.6 0.0 copy-start.1
  109.6 1.9 %copy.18 = bf16[128,2048]{1,0:T(8,128)(2,1)} copy(bf16[128,2048]{1,0:T(8,128)(2,1)} %get-tuple-element.10) | data formatting | bytes 1048576
  111.5 0.0 copy-done.1
  111.5 0.6 copy.19
  (3 shorter events, 0.0 us)
Async XLA Ops:
  0.6 3.1 %copy-start = (bf16[256,256]{1,0:T(8,128)(2,1)S(1)}, bf16[256,256]{1,0:T(8,128)(2,1)}, u32[]{:S(2)}) copy-start(bf16[256,256]{1,0:T(8,128)(2,1)} %param.14) | copy-start | bytes 393220
  109.6 1.9 %copy-start.1 = (f32[4,512]{1,0:T(4,128)S(1)}, f32[4,512]{1,0:T(4,128)}, u32[]{:S(2)}) copy-start(f32[4,512]{1,0:T(4,128)} %get-tuple-element.11) | copy-start | bytes 24580

commit v2 on v1

--- a/solution.py
+++ b/solution.py
@@ -1,4 +1,5 @@
 import functools
+import math
 
 import jax
 import jax.numpy as jnp
@@ -196,30 +197,18 @@
     return (mixed, log_weight_sum)
 
 
-def rope_tables(rows, lanes):
-    half_dim = HEAD_DIM // 2
-    positions = lax.axis_index("sp") * rows + jnp.arange(rows, dtype=jnp.int32)
-    lane = jnp.arange(lanes, dtype=jnp.int32) % HEAD_DIM
-    freq_index = lane % (half_dim // 2)
-    inv_freq = rope_base ** (-(2 * freq_index).astype(jnp.float32) / half_dim)
-    is_col = lane >= half_dim
-    index = jnp.where(is_col[None, :], (positions % GRID_W)[:, None], (positions // GRID_W)[:, None])
-    angle = index.astype(jnp.float32) * inv_freq[None, :]
-    sign = jnp.where((lane % half_dim) < half_dim // 2, -1.0, 1.0)
-    return jnp.cos(angle), jnp.sin(angle) * sign[None, :]
-
-
 def fused_kernel(
     Z, X,
-    tok_ref, gain_ref, win_ref, oa_ref, oc_ref, cos_ref, sin_ref, taps_ref, sink_ref,
+    tok_ref, gain_ref, wq_ref, wk_ref, wv_ref, wpost_ref, wpre_ref, wcin_ref, oa_ref, oc_ref, taps_ref, sink_ref,
     out_ref, lse_ref,
-    tok, normed, win, woa, woc, acc, qbuf, kvp, cf, chalo_out, chalo_in, att, cout,
+    cos_ref, sin_ref, tok, normed, win, woa, woc, acc, qbuf, kvp, cf, chalo_out, chalo_in, att, cout,
     part_keep, part_send, part_recv, y_send, y_recv,
     tok_sem, in_send, in_recv, oa_send, oa_recv, oc_send, oc_recv, halo_sem, rs_sem, loc_sem,
 ):
     S = Z * X
     rows, width = tok_ref.shape
-    depth = win_ref.shape[0]
+    depth = wq_ref.shape[0]
+    piece = depth // 2
     cols = oa_ref.shape[1]
     qw = qbuf.shape[1]
     cw = cf.shape[1]
@@ -235,6 +224,12 @@
     has_low, has_high = z > 0, z < Z - 1
     has_prev, has_next = sp > 0, sp < S - 1
 
+    kw = 2 * HEAD_DIM
+    win[sp, :, 0:qw] = wq_ref[...]
+    win[sp, :, qw:qw + kw] = jnp.concatenate([wk_ref[...], wv_ref[...]], axis=1)
+    for part, ref in enumerate((wpost_ref, wpre_ref, wcin_ref)):
+        win[sp, :, qw + kw + part * cw:qw + kw + (part + 1) * cw] = ref[...]
+
     barrier = pltpu.get_barrier_semaphore()
 
     def greet(dev):
@@ -260,23 +255,24 @@
 
     targets = (low, high, xnb)
 
+    def in_copy(slot, half, direction):
+        block = win.at[slot, pl.ds(half * piece, piece)]
+        return remote(
+            block, block, in_send.at[direction, half, slot], in_recv.at[half, slot], (targets[direction], tp)
+        )
+
     def weight_copy(kind, slot, direction, own=False):
-        buf, ssem, rsem, ref = (
-            (win, in_send, in_recv, win_ref),
-            (woa, oa_send, oa_recv, oa_ref),
-            (woc, oc_send, oc_recv, oc_ref),
-        )[kind]
+        buf, ssem, rsem, ref = ((woa, oa_send, oa_recv, oa_ref), (woc, oc_send, oc_recv, oc_ref))[kind - 1]
         source = ref if own else buf.at[slot]
         return remote(source, buf.at[slot], ssem.at[direction, slot], rsem.at[slot], (targets[direction], tp))
 
     weight_copy(2, sp, 2, True).start()
-    @pl.when(has_low)
-    def _():
-        weight_copy(0, sp, 0, True).start()
-    @pl.when(has_high)
-    def _():
-        weight_copy(0, sp, 1, True).start()
-    weight_copy(0, sp, 2, True).start()
+    for half in range(2):
+        for direction, cond in ((0, has_low), (1, has_high)):
+            @pl.when(cond)
+            def _(half=half, direction=direction):
+                in_copy(sp, half, direction).start()
+        in_copy(sp, half, 2).start()
 
     tok_y = remote(tok_ref, tok.at[tp], tok_sem.at[0], tok_sem.at[1], (sp, ynb))
     tok_y.start()
@@ -284,12 +280,27 @@
     tok_s.start()
     local = [
         pltpu.make_async_copy(tok_ref, tok.at[tp], loc_sem.at[0]),
-        pltpu.make_async_copy(win_ref, win.at[sp], loc_sem.at[1]),
         pltpu.make_async_copy(oa_ref, woa.at[sp], loc_sem.at[2]),
         pltpu.make_async_copy(oc_ref, woc.at[sp], loc_sem.at[3]),
     ]
     for copy in local:
         copy.start()
+
+    MB = 128
+    quarter = HEAD_DIM // 4
+
+    def angles(i, carry):
+        r = pl.ds(pl.multiple_of(i * MB, MB), MB)
+        pos = sp * rows + i * MB + lax.broadcasted_iota(jnp.int32, (MB, kw), 0)
+        lane = lax.broadcasted_iota(jnp.int32, (MB, kw), 1) % HEAD_DIM
+        freq = jnp.exp((lane % quarter).astype(jnp.float32) * (-4.0 / HEAD_DIM * math.log(rope_base)))
+        index = jnp.where(lane >= 2 * quarter, pos % GRID_W, pos // GRID_W)
+        angle = index.astype(jnp.float32) * freq
+        cos_ref[r, :] = jnp.cos(angle)
+        sin_ref[r, :] = jnp.where(lane % (2 * quarter) < quarter, -1.0, 1.0) * jnp.sin(angle)
+        return carry
+
+    lax.fori_loop(0, rows // MB, angles, 0)
     for copy in local:
         copy.wait()
     remote(tok.at[ynb], tok.at[ynb], tok_sem.at[0], tok_sem.at[1], (sp, ynb)).wait_recv()
@@ -316,8 +327,6 @@
 
     lax.fori_loop(0, rows // RB, norm_rows, 0)
 
-    MB = 128
-
     def project(slot, first):
         def body(i, carry):
             r = pl.ds(pl.multiple_of(i * MB, MB), MB)
@@ -366,56 +375,68 @@
 
     project(sp, True)
 
-    def in_step(k, carry):
-        zz, up, valid = entry(k)
-
-        @pl.when(valid & (k < entries))
-        def _():
-            slot = zz * X + x
-            wait_weight(0, slot)
-            pass_on(0, slot, up, True)
-            project(slot, False)
-
-        @pl.when(k == 2 * (Z - 2))
+    def out_comm(dist):
+        for kind, across, far in ((1, True, False), (2, False, False), (2, False, True)):
+            for up in (0, 1):
+                zz = z + dist * (2 * up - 1)
+
+                @pl.when((zz >= 0) & (zz < Z))
+                def _(zz=zz, up=up, kind=kind, across=across, far=far):
+                    slot = zz * X + (1 - x if far else x)
+                    wait_weight(kind, slot)
+                    pass_on(kind, slot, up, across)
+
+    def in_step(dist, carry):
+        for half in range(2):
+            for up in (0, 1):
+                zz = z + dist * (2 * up - 1)
+
+                @pl.when((zz >= 0) & (zz < Z))
+                def _(zz=zz, half=half, up=up):
+                    slot = zz * X + x
+                    in_copy(slot, half, 2).wait_recv()
+                    @pl.when(has_low if up else has_high)
+                    def _():
+                        in_copy(slot, half, 0 if up else 1).start()
+                    in_copy(slot, half, 2).start()
+
+        @pl.when(dist == Z - 2)
         def _():
             start_out_weights()
 
-        zo, _, valid_o = entry(k - 2)
-
-        @pl.when(valid_o & (k >= 2))
+        @pl.when(dist == Z - 1)
         def _():
-            slot = zo * X + 1 - x
-            wait_weight(0, slot)
-            project(slot, False)
+            out_comm(1)
+
+        def work(side, carry):
+            zz = z + dist * (2 * side - 1)
+
+            @pl.when((zz >= 0) & (zz < Z))
+            def _():
+                project(zz * X + x, False)
+            zo = z + (dist - 1) * (2 * side - 1)
+
+            @pl.when((zo >= 0) & (zo < Z) & ((dist > 1) | (side == 0)))
+            def _():
+                slot = zo * X + 1 - x
+                for half in range(2):
+                    in_copy(slot, half, 2).wait_recv()
+                project(slot, False)
+            return carry
+
+        lax.fori_loop(0, 2, work, 0)
         return carry
 
-    lax.fori_loop(1, entries + 2, in_step, 0)
-
-    def out_comm(dist):
-        for up in (0, 1):
-            zz = z + dist * (2 * up - 1)
-
-            @pl.when((zz >= 0) & (zz < Z))
-            def _(zz=zz, up=up):
-                mine, other = zz * X + x, zz * X + 1 - x
-                wait_weight(1, mine)
-                pass_on(1, mine, up, True)
-                wait_weight(2, mine)
-                pass_on(2, mine, up, False)
-                wait_weight(2, other)
-                pass_on(2, other, up, False)
+    lax.fori_loop(1, Z + 1, in_step, 0)
 
     def turned(v, cosv, sinv):
         lane = lax.broadcasted_iota(jnp.int32, v.shape, 1)
-        quarter = HEAD_DIM // 4
         partner = jnp.where(
             lane % (2 * quarter) < quarter,
             pltpu.roll(v, v.shape[1] - quarter, 1),
             pltpu.roll(v, quarter, 1),
         )
         return v * cosv + partner * sinv
-
-    kw = 2 * HEAD_DIM
 
     def kv_rows(i, carry):
         r = pl.ds(pl.multiple_of(i * MB, MB), MB)
@@ -452,7 +473,8 @@
         for copy in to_prev:
             copy.start()
 
-    out_comm(1)
+    if Z > 2:
+        out_comm(2)
 
     def q_rows(i, carry):
         r = pl.ds(pl.multiple_of(i * MB, MB), MB)
@@ -527,7 +549,7 @@
                     q, k_half[side], (((1,), (1,)), ((), ())), preferred_element_type=jnp.float32
                 ) * HEAD_DIM ** (-0.5)
                 s = jnp.where(allowed, s, -jnp.inf)
-                sink = sink_ref[h:h + 1, 0:1]
+                sink = sink_ref[h]
                 top = jnp.maximum(jnp.max(s, axis=1, keepdims=True), sink)
                 e = jnp.exp(s - top)
                 den = jnp.sum(e, axis=1, keepdims=True) + jnp.exp(sink - top)
@@ -539,12 +561,7 @@
         return carry
 
     blocks = rows // WINDOW
-    lax.fori_loop(0, blocks // 2, attend, 0)
-    if Z > 2:
-        out_comm(2)
-    lax.fori_loop(blocks // 2, blocks, attend, 0)
-    for dist in range(3, Z):
-        out_comm(dist)
+    lax.fori_loop(0, blocks, attend, 0)
 
     chunk = rows // TP
 
@@ -601,11 +618,13 @@
             wait_weight(1, slot)
         out_block(slot)
 
-    half_u = entries
-    each(project_out, 0, half_u)
-    each(lambda slot, k, side: y_block(slot), 0, half_u)
-    each(project_out, half_u, 2 * entries)
-    each(lambda slot, k, side: y_block(slot), half_u, 2 * entries)
+    early = min(6, 2 * entries)
+    each(project_out, 0, early)
+    each(lambda slot, k, side: y_block(slot), 0, early)
+    for dist in range(3, Z):
+        out_comm(dist)
+    each(project_out, early, 2 * entries)
+    each(lambda slot, k, side: y_block(slot), early, 2 * entries)
     each(lambda slot, k, side: finish(slot), 0, 2 * entries)
 
     tok_y.wait_send()
@@ -627,11 +646,13 @@
         for direction, cond in ((0, (zz >= z) & has_low), (1, (zz <= z) & has_high)):
             @pl.when(cond)
             def _(direction=direction):
-                weight_copy(0, mine, direction).wait_send()
+                in_copy(mine, 0, direction).wait_send()
+                in_copy(mine, 1, direction).wait_send()
                 weight_copy(1, mine, direction).wait_send()
                 weight_copy(2, mine, direction).wait_send()
                 weight_copy(2, other, direction).wait_send()
-        weight_copy(0, mine, 2).wait_send()
+        in_copy(mine, 0, 2).wait_send()
+        in_copy(mine, 1, 2).wait_send()
         weight_copy(1, mine, 2).wait_send()
         for slot in (mine, other):
             sib_copy(slot).wait_send()
@@ -655,22 +676,21 @@
     cols = w_out_attn.shape[1]
     heads = qw // HEAD_DIM
     kw = 2 * HEAD_DIM
-    joined = jnp.concatenate((w_query, w_key, w_value, w_post_gate, w_pre_gate, w_conv_in), axis=1)
-    nw = joined.shape[1]
-    cosv, sinv = rope_tables(rows, kw)
+    nw = qw + kw + 3 * cw
     chunk = rows // TP
     bf, f32 = jnp.bfloat16, jnp.float32
     dma = pltpu.SemaphoreType.DMA
-    sinks = jnp.broadcast_to(sink_logit[:, None], (heads, kw))
     return pl.pallas_call(
         functools.partial(fused_kernel, Z, X),
         out_shape=(
             jax.ShapeDtypeStruct((chunk, S * cols), bf),
             jax.ShapeDtypeStruct((heads, rows), f32),
         ),
-        in_specs=[pl.BlockSpec(memory_space=pltpu.VMEM)] * 9,
+        in_specs=[pl.BlockSpec(memory_space=pltpu.VMEM)] * 11 + [pl.BlockSpec(memory_space=pltpu.SMEM)],
         out_specs=(pl.BlockSpec(memory_space=pltpu.VMEM),) * 2,
         scratch_shapes=[
+            pltpu.VMEM((rows, kw), f32),
+            pltpu.VMEM((rows, kw), f32),
             pltpu.VMEM((TP, rows, width), bf),
             pltpu.VMEM((rows, TP * width), bf),
             pltpu.VMEM((S, depth, nw), bf),
@@ -690,7 +710,7 @@
             pltpu.VMEM((S, chunk, cols), bf),
             pltpu.VMEM((S, chunk, cols), bf),
             dma((6,)),
-            dma((3, S)), dma((S,)),
+            dma((3, 2, S)), dma((2, S)),
             dma((3, S)), dma((S,)),
             dma((3, S)), dma((S,)),
             dma((8,)),
@@ -700,7 +720,10 @@
         compiler_params=pltpu.CompilerParams(
             collective_id=0, has_side_effects=True, vmem_limit_bytes=60 * 1024 * 1024
         ),
-    )(tokens, norm_gain[None, :], joined, w_out_attn, w_out_conv, cosv, sinv, conv_taps, sinks)
+    )(
+        tokens, norm_gain[None, :], w_query, w_key, w_value, w_post_gate, w_pre_gate, w_conv_in,
+        w_out_attn, w_out_conv, conv_taps, sink_logit,
+    )
 
 
 def fits(
@@ -711,7 +734,7 @@
     return (
         TP == 4
         and S % 2 == 0
-        and S >= 4
+        and S >= 6
         and w_key.shape[1] == HEAD_DIM
         and w_query.shape[0] % 128 == 0
         and w_query.shape[1] % 128 == 0

time: 113 us -> 98.7 us (0.87)
  the two profiles are of different devices: /device:TPU:0 before, /device:TPU:17 now
where the time goes in v2:
time: 98.7 us; the launch traced here: 98.5 us
  Pallas kernels  93.1 us (94%)
  local copies, waits for them, and re-layouts  4.72 us (5%)
    pallas_call x1, Pallas kernels, fused(): pl.pallas_call(functools.partial(fused_kernel, Z, X), out_shape=(jax.Shap...  93.1 us
    unnamed x8, local copies, waits for them, and re-layouts  4.72 us

profile of v2, /device:TPU:17, one launch (start us, length us, event | category | flops | bytes accessed | tf_op | source)
XLA Modules:
  0.0 98.5 jit_solution(4045642814174188388)
XLA Ops:
  0.6 0.0 copy-start
  0.6 1.5 %copy.14.wk_ref = bf16[256,64]{1,0:T(8,128)(2,1)} copy(bf16[256,64]{0,1:T(8,128)(2,1)} %param.15) | data formatting | bytes 65536 | tf_op args[3]
  2.1 0.0 copy-done
  2.1 0.7 copy.15.wv_ref
  2.9 93.1 %shard_map.131 = (bf16[128,2048]{1,0:T(8,128)(2,1)}, f32[4,512]{1,0:T(4,128)}) custom-call(bf16[512,512]{1,0:T(8,128)(2,1)} %tok_ref.1, f32[1,2048]{1,0:T(1,128)} %bitcast.1, bf16[256,256]{1,0:T(8,128)(2,1)} %wq_ref.1, bf16[256,64]{1,0:T(8,128)(2,1)} %copy.14.wk_ref, bf16[256,64]{1,0:T(8,128)(2,1)} %copy.15.wv_ref, bf16[256,256]{1,0:T(8,128)(2,1)} %wpost_ref.1, ...), custom_call_target="tpu_custom_call" | custom-call | tf_op jit(solution)/shard_map/pallas_call | solution.py:683
  96.0 0.0 copy-start.1
  96.0 1.9 %copy.18 = bf16[128,2048]{1,0:T(8,128)(2,1)} copy(bf16[128,2048]{1,0:T(8,128)(2,1)} %get-tuple-element.4) | data formatting | bytes 1048576
  97.9 0.0 copy-done.1
  97.9 0.6 copy.19
Async XLA Ops:
  0.6 1.5 %copy-start = (bf16[256,64]{0,1:T(8,128)(2,1)S(1)}, bf16[256,64]{0,1:T(8,128)(2,1)}, u32[]{:S(2)}) copy-start(bf16[256,64]{0,1:T(8,128)(2,1)} %param.16) | copy-start | bytes 98308
  96.0 1.9 %copy-start.1 = (f32[4,512]{1,0:T(4,128)S(1)}, f32[4,512]{1,0:T(4,128)}, u32[]{:S(2)}) copy-start(f32[4,512]{1,0:T(4,128)} %get-tuple-element.5) | copy-start | bytes 24580

commit v3 on v2

--- a/solution.py
+++ b/solution.py
@@ -226,7 +226,8 @@
 
     kw = 2 * HEAD_DIM
     win[sp, :, 0:qw] = wq_ref[...]
-    win[sp, :, qw:qw + kw] = jnp.concatenate([wk_ref[...], wv_ref[...]], axis=1)
+    kv_t = jnp.concatenate([wk_ref[...], wv_ref[...]], axis=0).astype(jnp.float32)
+    win[sp, :, qw:qw + kw] = jnp.transpose(kv_t).astype(jnp.bfloat16)
     for part, ref in enumerate((wpost_ref, wpre_ref, wcin_ref)):
         win[sp, :, qw + kw + part * cw:qw + kw + (part + 1) * cw] = ref[...]
 
@@ -301,6 +302,22 @@
         return carry
 
     lax.fori_loop(0, rows // MB, angles, 0)
+
+    def in_comm(dist):
+        for half in range(2):
+            for up in (0, 1):
+                zz = z + dist * (2 * up - 1)
+
+                @pl.when((zz >= 0) & (zz < Z))
+                def _(zz=zz, half=half, up=up):
+                    slot = zz * X + x
+                    in_copy(slot, half, 2).wait_recv()
+                    @pl.when(has_low if up else has_high)
+                    def _():
+                        in_copy(slot, half, 0 if up else 1).start()
+                    in_copy(slot, half, 2).start()
+
+    in_comm(1)
     for copy in local:
         copy.wait()
     remote(tok.at[ynb], tok.at[ynb], tok_sem.at[0], tok_sem.at[1], (sp, ynb)).wait_recv()
@@ -387,18 +404,9 @@
                     pass_on(kind, slot, up, across)
 
     def in_step(dist, carry):
-        for half in range(2):
-            for up in (0, 1):
-                zz = z + dist * (2 * up - 1)
-
-                @pl.when((zz >= 0) & (zz < Z))
-                def _(zz=zz, half=half, up=up):
-                    slot = zz * X + x
-                    in_copy(slot, half, 2).wait_recv()
-                    @pl.when(has_low if up else has_high)
-                    def _():
-                        in_copy(slot, half, 0 if up else 1).start()
-                    in_copy(slot, half, 2).start()
+        @pl.when(dist > 1)
+        def _():
+            in_comm(dist)
 
         @pl.when(dist == Z - 2)
         def _():
@@ -621,10 +629,12 @@
     early = min(6, 2 * entries)
     each(project_out, 0, early)
     each(lambda slot, k, side: y_block(slot), 0, early)
-    for dist in range(3, Z):
-        out_comm(dist)
-    each(project_out, early, 2 * entries)
-    each(lambda slot, k, side: y_block(slot), early, 2 * entries)
+    for dist in range(2, Z):
+        if dist > 2:
+            out_comm(dist)
+        lo, hi = 4 * dist - 2, 4 * dist + 2
+        each(project_out, lo, hi)
+        each(lambda slot, k, side: y_block(slot), lo, hi)
     each(lambda slot, k, side: finish(slot), 0, 2 * entries)
 
     tok_y.wait_send()
@@ -721,7 +731,7 @@
             collective_id=0, has_side_effects=True, vmem_limit_bytes=60 * 1024 * 1024
         ),
     )(
-        tokens, norm_gain[None, :], w_query, w_key, w_value, w_post_gate, w_pre_gate, w_conv_in,
+        tokens, norm_gain[None, :], w_query, w_key.T, w_value.T, w_post_gate, w_pre_gate, w_conv_in,
         w_out_attn, w_out_conv, conv_taps, sink_logit,
     )
 

time: 98.7 us -> 95.7 us (0.970)
  local copies, waits for them, and re-layouts: 4.72 us -> 2.49 us
  Pallas kernels: 93.1 us -> 91.6 us
    unnamed x8 -> x4, local copies, waits for them, and re-layouts: 4.72 us -> 2.49 us
    pallas_call x1, Pallas kernels: 93.1 us -> 91.6 us  [fused(): pl.pallas_call(functools.partial(fused_kernel, Z, X), out_shape=(jax.Shap...]
where the time goes in v3:
time: 95.7 us; the launch traced here: 94.7 us
  Pallas kernels  91.6 us (96%)
  local copies, waits for them, and re-layouts  2.49 us (3%)
    pallas_call x1, Pallas kernels, fused(): pl.pallas_call(functools.partial(fused_kernel, Z, X), out_shape=(jax.Shap...  91.6 us
    unnamed x4, local copies, waits for them, and re-layouts  2.49 us

profile of v3, /device:TPU:17, one launch (start us, length us, event | category | flops | bytes accessed | tf_op | source)
XLA Modules:
  0.0 94.7 jit_solution(13633581503702134390)
XLA Ops:
  0.6 91.6 %shard_map.131 = (bf16[128,2048]{1,0:T(8,128)(2,1)}, f32[4,512]{1,0:T(4,128)}) custom-call(bf16[512,512]{1,0:T(8,128)(2,1)} %tok_ref.1, f32[1,2048]{1,0:T(1,128)} %bitcast.5, bf16[256,256]{1,0:T(8,128)(2,1)} %wq_ref.1, bf16[64,256]{1,0:T(8,128)(2,1)} %bitcast.3, bf16[64,256]{1,0:T(8,128)(2,1)} %bitcast.4, bf16[256,256]{1,0:T(8,128)(2,1)} %wpost_ref.1, ...), custom_call_target="tpu_custom_call" | custom-call | tf_op jit(solution)/shard_map/pallas_call | solution.py:693
  92.2 0.0 copy-start
  92.2 1.9 %copy.16 = bf16[128,2048]{1,0:T(8,128)(2,1)} copy(bf16[128,2048]{1,0:T(8,128)(2,1)} %get-tuple-element.4) | data formatting | bytes 1048576
  94.1 0.0 copy-done
  94.1 0.6 copy.17
Async XLA Ops:
  92.2 1.9 %copy-start = (f32[4,512]{1,0:T(4,128)S(1)}, f32[4,512]{1,0:T(4,128)}, u32[]{:S(2)}) copy-start(f32[4,512]{1,0:T(4,128)} %get-tuple-element.5) | copy-start | bytes 24580
